TPU v7x, 32 devices: a whole 2x2x4 slice. The times are simulated.
32 devices in a mesh: fs: 8 (over z, y), tp: 4 (over x, core).
Axes of the slice: x: 2, y: 2, z: 4, core: 2. Of those that a mesh axis runs over, the one named last changes fastest.
Arguments:
- tokens: bfloat16 [8192, 2048], P('fs'), may hold values from -6 to 6
- norm_gain: float32 [2048], replicated, may hold values from 0.1 to 1.9
- gate_weight: bfloat16 [2048, 4096], P('fs', 'tp'), may hold values from -0.125 to 0.125
- up_weight: bfloat16 [2048, 4096], P('fs', 'tp'), may hold values from -0.125 to 0.125
- down_weight: bfloat16 [4096, 2048], P('tp', 'fs'), may hold values from -2 to 2
- out_gain: float32 [2048], P('tp'), may hold values from 0.1 to 1.9
Outputs:
- result: bfloat16 [8192, 2048], P('fs', 'tp')
All inputs are finite; a program needn't handle non-finite values.
Results may differ from a plain program's by a relative error of at most 0.014.
Values may be sent and summed in bfloat16 or wider, within the bound.
No kernel may reach another device: no remote copies, remote signals or barrier semaphores. Data moves between devices by JAX's collectives and lax.ppermute only.
A program may use at most 64 MiB of HBM per device.

v0:
```python
import jax
import jax.numpy as jnp
from jax import lax
from jax.sharding import PartitionSpec as P

EPSILON = 1e-06


def body(tokens, norm_gain, gate_weight, up_weight, down_weight, out_gain):
    values = tokens.astype(jnp.float32)
    normed = (
        values * lax.rsqrt(jnp.mean(values * values, axis=1, keepdims=True) + EPSILON) * norm_gain
    ).astype(jnp.bfloat16)
    gate_all, up_all = (
        lax.all_gather(gate_weight, "fs", axis=0, tiled=True),
        lax.all_gather(up_weight, "fs", axis=0, tiled=True),
    )
    gate_proj = jnp.dot(normed, gate_all, preferred_element_type=jnp.float32)
    up_proj = jnp.dot(normed, up_all, preferred_element_type=jnp.float32)
    hidden = (jax.nn.silu(gate_proj) * up_proj).astype(jnp.bfloat16)
    partial_value = jnp.dot(
        hidden,
        lax.all_gather(down_weight, "fs", axis=1, tiled=True),
        preferred_element_type=jnp.float32,
    )
    own_width = out_gain.shape[0]
    own_columns = lax.psum_scatter(
        partial_value.astype(jnp.bfloat16), "tp", scatter_dimension=1, tiled=True
    ).astype(jnp.float32)
    squares = lax.psum(jnp.sum(own_columns * own_columns, axis=1), "tp")
    mean_square = squares / (own_width * lax.axis_size("tp"))
    scaled = own_columns * lax.rsqrt(mean_square + EPSILON)[:, None] * out_gain[None, :]
    return scaled.astype(jnp.bfloat16)


def solution(mesh):
    return jax.shard_map(
        body,
        mesh=mesh,
        in_specs=(P("fs", None), P(), P("fs", "tp"), P("fs", "tp"), P("tp", "fs"), P("tp")),
        out_specs=P("fs", "tp"),
        check_vma=False,
    )
```

profile of v0, /device:TPU:0, one launch (start us, length us, event | category | flops | bytes accessed | tf_op | source)
XLA Modules:
  0.0 308.2 jit_solution(11775894596299125198)
XLA Ops:
  6.5 0.0 copy-start.1
  6.5 0.0 all-gather.4.cloned.1.call-start
  6.5 0.7 all-gather.4.cloned.1.call-update
  7.3 0.0 all-gather.6.cloned.1.call-start
  7.3 0.7 all-gather.6.cloned.1.call-update
  8.0 0.0 all-gather.8.cloned.1.call-start
  8.1 0.7 all-gather.8.cloned.1.call-update
  8.7 0.0 reduce-scatter.2.cloned.1.call-start
  8.8 3.1 fusion
  11.9 73.1 %all-gather.4.cloned.1.call-done = bf16[2048,1024]{1,0:T(8,128)(2,1)} async-done(((bf16[256,1024]{1,0:T(8,128)(2,1)}), bf16[2048,1024]{1,0:T(8,128)(2,1)}) %all-gather.4.cloned.1.call-update) | async-done | bytes 4194320 | tf_op jit(solution)/shard_map/all_gather | solution.py:15
  85.0 0.0 copy-done.1
  85.0 10.0 %fusion.7 = f32[1024,1024]{1,0:T(8,128)} fusion(bf16[2048,1024]{1,0:T(8,128)(2,1)} %all-gather.4.cloned.1.call-done, bf16[1024,2048]{1,0:T(8,128)(2,1)} %param.6, f32[2048]{0:T(1024)S(1)} %copy-done.1, f32[1024]{0:T(1024)S(1)} %add_rsqrt_fusion.1), kind=kOutput, calls=%fused_computation.12 | convolution fusion | flops 4303355904 | bytes 12595200 | tf_op jit(solution)/shard_map/dot_general | solution.py:18
  95.0 63.5 %all-gather.6.cloned.1.call-done = bf16[2048,1024]{1,0:T(8,128)(2,1)} async-done(((bf16[256,1024]{1,0:T(8,128)(2,1)}), bf16[2048,1024]{1,0:T(8,128)(2,1)}) %all-gather.6.cloned.1.call-update) | async-done | bytes 4194320 | tf_op jit(solution)/shard_map/all_gather | solution.py:16
  158.5 75.3 %all-gather.8.cloned.1.call-done = bf16[1024,2048]{1,0:T(8,128)(2,1)} async-done(((bf16[1024,256]{1,0:T(8,128)(2,1)}), bf16[1024,2048]{1,0:T(8,128)(2,1)}) %all-gather.8.cloned.1.call-update) | async-done | bytes 4194320 | tf_op jit(solution)/shard_map/all_gather | solution.py:23
  233.7 15.3 %convolution_convert_fusion = bf16[1024,2048]{1,0:T(8,128)(2,1)} fusion(bf16[1024,2048]{1,0:T(8,128)(2,1)} %all-gather.8.cloned.1.call-done, f32[1024,1024]{1,0:T(8,128)} %fusion.7, bf16[2048,1024]{1,0:T(8,128)(2,1)} %all-gather.6.cloned.1.call-done, bf16[1024,2048]{1,0:T(8,128)(2,1)} %param.6, f32[2048]{0:T(1024)S(1)} %copy-done.1, ...), kind=kOutput, calls=%fused_computation.6 | convolution fusion | flops 8606711808 | bytes 20983808 | tf_op jit(solution)/shard_map/dot_general | solution.py:21
  249.1 0.0 copy-start
  249.1 0.0 reduce-scatter.2.cloned.1.call-update
  249.1 42.7 %reduce-scatter.2.cloned.1.call-done = bf16[1024,512]{1,0:T(8,128)(2,1)} async-done(((bf16[1024,2048]{1,0:T(8,128)(2,1)}), bf16[1024,512]{1,0:T(8,128)(2,1)}) %reduce-scatter.2.cloned.1.call-update) | async-done | bytes 1048592 | tf_op jit(solution)/shard_map/reduce_scatter | solution.py:27
  291.9 1.5 fusion.3
  293.4 5.8 %psum.7 = f32[1024]{0:T(1024)S(1)} all-reduce(f32[1024]{0:T(1024)S(1)} %fusion.3), channel_id=1, replica_groups=mesh['fs'=8,'tp'=4] {'tp'}, use_global_device_ids=true, to_apply=%region_3.4 | all-reduce | flops 1024 | bytes 8192 | tf_op jit(solution)/shard_map/psum | solution.py:30
  299.1 0.0 copy-done
  299.1 2.5 fusion.5
  (2 shorter events, 0.0 us)
Async XLA Ops:
  6.5 78.5 %copy-start.1 = (f32[2048]{0:T(1024)S(1)}, f32[2048]{0:T(1024)}, u32[]{:S(2)}) copy-start(f32[2048]{0:T(1024)} %param.7) | copy-start | bytes 24580
  6.5 78.5 %all-gather.4.cloned.1.call-start = ((), (), s32[]{:S(2)}) async-start(), calls=%async_computation.1 | async-start | bytes 4718592 | tf_op jit(solution)/shard_map/all_gather | solution.py:15
  7.3 151.2 %all-gather.6.cloned.1.call-start = ((), (), s32[]{:S(2)}) async-start(), calls=%async_computation.2 | async-start | bytes 4718592 | tf_op jit(solution)/shard_map/all_gather | solution.py:16
  8.0 225.7 %all-gather.8.cloned.1.call-start = ((), (), s32[]{:S(2)}) async-start(), calls=%async_computation.3 | async-start | bytes 4718592 | tf_op jit(solution)/shard_map/all_gather | solution.py:23
  8.7 283.1 %reduce-scatter.2.cloned.1.call-start = ((), (), s32[]{:S(2)}) async-start(), calls=%async_computation.4 | async-start | bytes 5242880 | tf_op jit(solution)/shard_map/reduce_scatter | solution.py:27
  249.1 50.0 %copy-start = (f32[512]{0:T(512)S(1)}, f32[512]{0:T(512)}, u32[]{:S(2)}) copy-start(f32[512]{0:T(512)} %param.11) | copy-start | bytes 6148
Sparse Core Ops, SparseCore 0:
  9.5 75.5 all-gather.3
  87.1 71.3 all-gather.5
  160.5 73.1 all-gather.7
  249.2 42.5 reduce-scatter.1
where the time goes:
time: 308 us
  waiting for transfers between devices  257 us (83%)
  matrix products  25.3 us (8%)
  between operations  13.1 us (4%)
  other arithmetic  7.09 us (2%)
  blocking collectives  5.77 us (2%)
    all_gather x1, waiting for transfers between devices, body(): lax.all_gather(down_weight, 'fs', axis=1, tiled=True)  75.3 us
    all_gather x1, waiting for transfers between devices, body(): lax.all_gather(gate_weight, 'fs', axis=0, tiled=True)  73.1 us
    all_gather x1, waiting for transfers between devices, body(): lax.all_gather(up_weight, 'fs', axis=0, tiled=True)  63.5 us
    reduce_scatter x1, waiting for transfers between devices, body(): lax.psum_scatter(partial_value.astype(jnp.bfloat16), 'tp', scatter_dimens...  42.7 us
    dot_general x1, matrix products, body(): jnp.dot(hidden, lax.all_gather(down_weight, 'fs', axis=1, tiled=True), pr...  15.3 us
    dot_general x1, matrix products, body(): gate_proj = jnp.dot(normed, gate_all, preferred_element_type=jnp.float32)  9.96 us
  transfers between devices with their start and end apart: 4, of which 4 were waited for; matrix products, arithmetic and copies ran while one was open for 4% of the time, Pallas kernels for 0%

commit v1 on v0

--- a/solution.py
+++ b/solution.py
@@ -11,8 +11,23 @@
     normed = (
         values * lax.rsqrt(jnp.mean(values * values, axis=1, keepdims=True) + EPSILON) * norm_gain
     ).astype(jnp.bfloat16)
+
+    def wait_tasks(local):
+        n_all = lax.axis_size("fs")
+        views = [local]
+        ix = 1
+        while ix < n_all:
+            views.append(
+                lax.ppermute(views[ix - 1], "fs", perm=[(w, (w - 1) % n_all) for w in range(n_all)])
+            )
+            ix += 1
+        part_next = jnp.concatenate(views, axis=0)
+        before = lax.axis_index("fs")
+        carry = jnp.roll(part_next, before * local.shape[0], 0)
+        return carry
+
     gate_all, up_all = (
-        lax.all_gather(gate_weight, "fs", axis=0, tiled=True),
+        wait_tasks(gate_weight),
         lax.all_gather(up_weight, "fs", axis=0, tiled=True),
     )
     gate_proj = jnp.dot(normed, gate_all, preferred_element_type=jnp.float32)

time: 308 us -> 288 us (0.935)
  waiting for transfers between devices: 257 us -> 182 us
  starting transfers between devices: 0.12 us -> 37.3 us
  local copies, waits for them, and re-layouts: 0.01 us -> 16.5 us
    ppermute x0 -> x7, waiting for transfers between devices: none -> 106 us  [wait_tasks(): lax.ppermute(views[ix - 1], 'fs', perm=[(w, (w - 1) % n_all) for w in ran...]
    all_gather x1 -> x0, waiting for transfers between devices: 73.1 us -> none  [body(): lax.all_gather(gate_weight, 'fs', axis=0, tiled=True)]
    all_gather x1, waiting for transfers between devices: 63.5 us -> 0.01 us  [body(): lax.all_gather(up_weight, 'fs', axis=0, tiled=True)]
    all_gather x1, waiting for transfers between devices: 75.3 us -> 31.7 us  [body(): lax.all_gather(down_weight, 'fs', axis=1, tiled=True)]
    ppermute x0 -> x7, starting transfers between devices: none -> 37.2 us  [wait_tasks(): lax.ppermute(views[ix - 1], 'fs', perm=[(w, (w - 1) % n_all) for w in ran...]
    unnamed x4 -> x21, local copies, waits for them, and re-layouts: 0.01 us -> 15.6 us
  transfers between devices with their start and end apart: 4 -> 10, of which waited for: 4 -> 9; matrix products, arithmetic and copies ran while one was open for 4% -> 10% of each run, Pallas kernels for 0% -> 0%
where the time goes in v1:
time: 288 us
  waiting for transfers between devices  182 us (63%)
  starting transfers between devices  37.3 us (13%)
  matrix products  25.7 us (9%)
  local copies, waits for them, and re-layouts  16.5 us (6%)
  between operations  13.2 us (5%)
  other arithmetic  7.09 us (2%)
  blocking collectives  5.77 us (2%)
    ppermute x7, waiting for transfers between devices, wait_tasks(): lax.ppermute(views[ix - 1], 'fs', perm=[(w, (w - 1) % n_all) for w in ran...  106 us
    reduce_scatter x1, waiting for transfers between devices, body(): lax.psum_scatter(partial_value.astype(jnp.bfloat16), 'tp', scatter_dimens...  42.8 us
    ppermute x7, starting transfers between devices, wait_tasks(): lax.ppermute(views[ix - 1], 'fs', perm=[(w, (w - 1) % n_all) for w in ran...  37.2 us
    all_gather x1, waiting for transfers between devices, body(): lax.all_gather(down_weight, 'fs', axis=1, tiled=True)  31.7 us
    dot_general x1, matrix products, body(): jnp.dot(hidden, lax.all_gather(down_weight, 'fs', axis=1, tiled=True), pr...  15.6 us
    unnamed x21, local copies, waits for them, and re-layouts  15.6 us
    dot_general x1, matrix products, body(): up_proj = jnp.dot(normed, up_all, preferred_element_type=jnp.float32)  10.1 us
    psum x1, blocking collectives, body(): squares = lax.psum(jnp.sum(own_columns * own_columns, axis=1), 'tp')  5.77 us
  transfers between devices with their start and end apart: 10, of which 9 were waited for; matrix products, arithmetic and copies ran while one was open for 10% of the time, Pallas kernels for 0%

profile of v1, /device:TPU:0, one launch (start us, length us, event | category | flops | bytes accessed | tf_op | source)
XLA Modules:
  0.0 287.7 jit_solution(12533305621783459778)
XLA Ops:
  8.1 6.1 %collective-permute-start = (bf16[256,1024]{1,0:T(8,128)(2,1)}, bf16[256,1024]{1,0:T(8,128)(2,1)S(1)}, u32[]{:S(2)}, u32[]{:S(2)}) collective-permute-start(bf16[256,1024]{1,0:T(8,128)(2,1)} %param.8), channel_id=1, source_target_pairs={{0,28},{4,0},{8,4},{12,8},{16,12},{20,16},{24,20},{28,24},{1,29},{... | collective-permute-start | bytes 1572872 | tf_op jit(solution)/shard_map/ppermute | solution.py:21
  14.1 17.0 %collective-permute-done = bf16[256,1024]{1,0:T(8,128)(2,1)S(1)} collective-permute-done((bf16[256,1024]{1,0:T(8,128)(2,1)}, bf16[256,1024]{1,0:T(8,128)(2,1)S(1)}, u32[]{:S(2)}, u32[]{:S(2)}) %collective-permute-start) | collective-permute-done | bytes 524320 | tf_op jit(solution)/shard_map/ppermute | solution.py:21
  31.2 5.1 %collective-permute-start.1 = (bf16[256,1024]{1,0:T(8,128)(2,1)S(1)}, bf16[256,1024]{1,0:T(8,128)(2,1)S(1)}, u32[]{:S(2)}, u32[]{:S(2)}) collective-permute-start(bf16[256,1024]{1,0:T(8,128)(2,1)S(1)} %collective-permute-done), channel_id=1, source_target_pairs={{0,28},{4,0},{8,4},{12,8},{16,12},{20,16},{24,20},{28,24},{1,29},{... | collective-permute-start | bytes 1572872 | tf_op jit(solution)/shard_map/ppermute | solution.py:21
  36.3 17.4 %collective-permute-done.1 = bf16[256,1024]{1,0:T(8,128)(2,1)S(1)} collective-permute-done((bf16[256,1024]{1,0:T(8,128)(2,1)S(1)}, bf16[256,1024]{1,0:T(8,128)(2,1)S(1)}, u32[]{:S(2)}, u32[]{:S(2)}) %collective-permute-start.1) | collective-permute-done | bytes 524320 | tf_op jit(solution)/shard_map/ppermute | solution.py:21
  53.6 5.2 %collective-permute-start.2 = (bf16[256,1024]{1,0:T(8,128)(2,1)S(1)}, bf16[256,1024]{1,0:T(8,128)(2,1)S(1)}, u32[]{:S(2)}, u32[]{:S(2)}) collective-permute-start(bf16[256,1024]{1,0:T(8,128)(2,1)S(1)} %collective-permute-done.1), channel_id=1, source_target_pairs={{0,28},{4,0},{8,4},{12,8},{16,12},{20,16},{24,20},{28,24},{1,29},{... | collective-permute-start | bytes 1572872 | tf_op jit(solution)/shard_map/ppermute | solution.py:21
  58.8 21.4 %collective-permute-done.2 = bf16[256,1024]{1,0:T(8,128)(2,1)S(1)} collective-permute-done((bf16[256,1024]{1,0:T(8,128)(2,1)S(1)}, bf16[256,1024]{1,0:T(8,128)(2,1)S(1)}, u32[]{:S(2)}, u32[]{:S(2)}) %collective-permute-start.2) | collective-permute-done | bytes 524320 | tf_op jit(solution)/shard_map/ppermute | solution.py:21
  80.2 5.2 %collective-permute-start.3 = (bf16[256,1024]{1,0:T(8,128)(2,1)S(1)}, bf16[256,1024]{1,0:T(8,128)(2,1)S(1)}, u32[]{:S(2)}, u32[]{:S(2)}) collective-permute-start(bf16[256,1024]{1,0:T(8,128)(2,1)S(1)} %collective-permute-done.2), channel_id=1, source_target_pairs={{0,28},{4,0},{8,4},{12,8},{16,12},{20,16},{24,20},{28,24},{1,29},{... | collective-permute-start | bytes 1572872 | tf_op jit(solution)/shard_map/ppermute | solution.py:21
  85.4 21.7 %collective-permute-done.3 = bf16[256,1024]{1,0:T(8,128)(2,1)S(1)} collective-permute-done((bf16[256,1024]{1,0:T(8,128)(2,1)S(1)}, bf16[256,1024]{1,0:T(8,128)(2,1)S(1)}, u32[]{:S(2)}, u32[]{:S(2)}) %collective-permute-start.3) | collective-permute-done | bytes 524320 | tf_op jit(solution)/shard_map/ppermute | solution.py:21
  107.2 5.2 %collective-permute-start.4 = (bf16[256,1024]{1,0:T(8,128)(2,1)S(1)}, bf16[256,1024]{1,0:T(8,128)(2,1)S(1)}, u32[]{:S(2)}, u32[]{:S(2)}) collective-permute-start(bf16[256,1024]{1,0:T(8,128)(2,1)S(1)} %collective-permute-done.3), channel_id=1, source_target_pairs={{0,28},{4,0},{8,4},{12,8},{16,12},{20,16},{24,20},{28,24},{1,29},{... | collective-permute-start | bytes 1572872 | tf_op jit(solution)/shard_map/ppermute | solution.py:21
  112.4 12.7 %collective-permute-done.4 = bf16[256,1024]{1,0:T(8,128)(2,1)S(1)} collective-permute-done((bf16[256,1024]{1,0:T(8,128)(2,1)S(1)}, bf16[256,1024]{1,0:T(8,128)(2,1)S(1)}, u32[]{:S(2)}, u32[]{:S(2)}) %collective-permute-start.4) | collective-permute-done | bytes 524320 | tf_op jit(solution)/shard_map/ppermute | solution.py:21
  125.1 5.2 %collective-permute-start.5 = (bf16[256,1024]{1,0:T(8,128)(2,1)S(1)}, bf16[256,1024]{1,0:T(8,128)(2,1)}, u32[]{:S(2)}, u32[]{:S(2)}) collective-permute-start(bf16[256,1024]{1,0:T(8,128)(2,1)S(1)} %collective-permute-done.4), channel_id=1, source_target_pairs={{0,28},{4,0},{8,4},{12,8},{16,12},{20,16},{24,20},{28,24},{1,29},{... | collective-permute-start | bytes 1572872 | tf_op jit(solution)/shard_map/ppermute | solution.py:21
  130.3 3.1 %fusion = f32[1024]{0:T(1024)S(1)} fusion(bf16[1024,2048]{1,0:T(8,128)(2,1)} %param.6), kind=kLoop, calls=%fused_computation.2 | loop fusion | flops 6290432 | bytes 4198400 | tf_op jit(solution)/shard_map/reduce_sum | solution.py:12
  133.4 1.9 constant_dynamic-update-slice_fusion.15
  136.1 8.3 %collective-permute-done.5 = bf16[256,1024]{1,0:T(8,128)(2,1)} collective-permute-done((bf16[256,1024]{1,0:T(8,128)(2,1)S(1)}, bf16[256,1024]{1,0:T(8,128)(2,1)}, u32[]{:S(2)}, u32[]{:S(2)}) %collective-permute-start.5) | collective-permute-done | bytes 524320 | tf_op jit(solution)/shard_map/ppermute | solution.py:21
  144.4 5.3 %collective-permute-start.6 = (bf16[256,1024]{1,0:T(8,128)(2,1)}, bf16[256,1024]{1,0:T(8,128)(2,1)S(1)}, u32[]{:S(2)}, u32[]{:S(2)}) collective-permute-start(bf16[256,1024]{1,0:T(8,128)(2,1)} %collective-permute-done.5), channel_id=1, source_target_pairs={{0,28},{4,0},{8,4},{12,8},{16,12},{20,16},{24,20},{28,24},{1,29},{... | collective-permute-start | bytes 1572872 | tf_op jit(solution)/shard_map/ppermute | solution.py:21
  153.1 1.9 constant_dynamic-update-slice_fusion.9
  154.9 7.7 %collective-permute-done.6 = bf16[256,1024]{1,0:T(8,128)(2,1)S(1)} collective-permute-done((bf16[256,1024]{1,0:T(8,128)(2,1)}, bf16[256,1024]{1,0:T(8,128)(2,1)S(1)}, u32[]{:S(2)}, u32[]{:S(2)}) %collective-permute-start.6) | collective-permute-done | bytes 524320 | tf_op jit(solution)/shard_map/ppermute | solution.py:21
  168.4 1.9 constant_dynamic-update-slice_fusion.1
  171.1 10.1 %fusion.13 = f32[1024,1024]{1,0:T(8,128)} fusion(bf16[2048,1024]{1,0:T(8,128)(2,1)} %all-gather.3.cloned.1.call-done, bf16[1024,2048]{1,0:T(8,128)(2,1)} %param.6, f32[2048]{0:T(1024)S(1)} %copy-done.2, f32[1024]{0:T(1024)S(1)} %add_rsqrt_fusion.1), kind=kOutput, calls=%fused_computation.15 | convolution fusion | flops 4303355904 | bytes 12595200 | tf_op jit(solution)/shard_map/dot_general | solution.py:34
  181.2 31.7 %all-gather.5.cloned.1.call-done = bf16[1024,2048]{1,0:T(8,128)(2,1)} async-done(((bf16[1024,256]{1,0:T(8,128)(2,1)}), bf16[1024,2048]{1,0:T(8,128)(2,1)}) %all-gather.5.cloned.1.call-update) | async-done | bytes 4194320 | tf_op jit(solution)/shard_map/all_gather | solution.py:38
  213.0 15.6 %convolution_convert_fusion = bf16[1024,2048]{1,0:T(8,128)(2,1)} fusion(bf16[1024,2048]{1,0:T(8,128)(2,1)} %all-gather.5.cloned.1.call-done, f32[1024,1024]{1,0:T(8,128)} %fusion.13, bf16[4096,1024]{1,0:T(8,128)(2,1)} %constant_dynamic-update-slice_fusion, s32[]{:T(128)S(6)} %select_n.14, bf16[1024,2048]{1,0:T(8,128)(2,1)} %param.6, f32[2048]{0:T(1024)S(1)} %copy-done.2, ...), kind=kOutput, calls=%fused_computation.8 | convolution fusion | flops 8606711808 | bytes 20983812 | tf_op jit(solution)/shard_map/dot_general | solution.py:36
  228.6 42.8 %reduce-scatter.2.cloned.1.call-done = bf16[1024,512]{1,0:T(8,128)(2,1)} async-done(((bf16[1024,2048]{1,0:T(8,128)(2,1)}), bf16[1024,512]{1,0:T(8,128)(2,1)}) %reduce-scatter.2.cloned.1.call-update) | async-done | bytes 1048592 | tf_op jit(solution)/shard_map/reduce_scatter | solution.py:42
  272.9 5.8 %psum.7 = f32[1024]{0:T(1024)S(1)} all-reduce(f32[1024]{0:T(1024)S(1)} %fusion.9), channel_id=1, replica_groups=mesh['fs'=8,'tp'=4] {'tp'}, use_global_device_ids=true, to_apply=%region_3.4 | all-reduce | flops 1024 | bytes 8192 | tf_op jit(solution)/shard_map/psum | solution.py:45
  278.7 2.5 fusion.11
  (29 shorter events, 13.9 us)
Async XLA Ops:
  6.5 156.9 %copy-start = (bf16[256,1024]{1,0:T(8,128)(2,1)S(1)}, bf16[256,1024]{1,0:T(8,128)(2,1)}, u32[]{:S(2)}) copy-start(bf16[256,1024]{1,0:T(8,128)(2,1)} %param.8) | copy-start | bytes 1572868
  6.5 164.6 %all-gather.3.cloned.1.call-start = ((), (), s32[]{:S(2)}) async-start(), calls=%async_computation.1 | async-start | bytes 4718592 | tf_op jit(solution)/shard_map/all_gather | solution.py:31
  7.3 205.7 %all-gather.5.cloned.1.call-start = ((), (), s32[]{:S(2)}) async-start(), calls=%async_computation.2 | async-start | bytes 4718592 | tf_op jit(solution)/shard_map/all_gather | solution.py:38
  8.0 263.4 %reduce-scatter.2.cloned.1.call-start = ((), (), s32[]{:S(2)}) async-start(), calls=%async_computation.3 | async-start | bytes 5242880 | tf_op jit(solution)/shard_map/reduce_scatter | solution.py:42
  8.1 23.1 %collective-permute-start = (bf16[256,1024]{1,0:T(8,128)(2,1)}, bf16[256,1024]{1,0:T(8,128)(2,1)S(1)}, u32[]{:S(2)}, u32[]{:S(2)}) collective-permute-start(bf16[256,1024]{1,0:T(8,128)(2,1)} %param.8), channel_id=1, source_target_pairs={{0,28},{4,0},{8,4},{12,8},{16,12},{20,16},{24,20},{28,24},{1,29},{... | collective-permute-start | bytes 1572872 | tf_op jit(solution)/shard_map/ppermute | solution.py:21
  31.2 22.4 %collective-permute-start.1 = (bf16[256,1024]{1,0:T(8,128)(2,1)S(1)}, bf16[256,1024]{1,0:T(8,128)(2,1)S(1)}, u32[]{:S(2)}, u32[]{:S(2)}) collective-permute-start(bf16[256,1024]{1,0:T(8,128)(2,1)S(1)} %collective-permute-done), channel_id=1, source_target_pairs={{0,28},{4,0},{8,4},{12,8},{16,12},{20,16},{24,20},{28,24},{1,29},{... | collective-permute-start | bytes 1572872 | tf_op jit(solution)/shard_map/ppermute | solution.py:21
  53.6 26.6 %collective-permute-start.2 = (bf16[256,1024]{1,0:T(8,128)(2,1)S(1)}, bf16[256,1024]{1,0:T(8,128)(2,1)S(1)}, u32[]{:S(2)}, u32[]{:S(2)}) collective-permute-start(bf16[256,1024]{1,0:T(8,128)(2,1)S(1)} %collective-permute-done.1), channel_id=1, source_target_pairs={{0,28},{4,0},{8,4},{12,8},{16,12},{20,16},{24,20},{28,24},{1,29},{... | collective-permute-start | bytes 1572872 | tf_op jit(solution)/shard_map/ppermute | solution.py:21
  80.2 26.9 %collective-permute-start.3 = (bf16[256,1024]{1,0:T(8,128)(2,1)S(1)}, bf16[256,1024]{1,0:T(8,128)(2,1)S(1)}, u32[]{:S(2)}, u32[]{:S(2)}) collective-permute-start(bf16[256,1024]{1,0:T(8,128)(2,1)S(1)} %collective-permute-done.2), channel_id=1, source_target_pairs={{0,28},{4,0},{8,4},{12,8},{16,12},{20,16},{24,20},{28,24},{1,29},{... | collective-permute-start | bytes 1572872 | tf_op jit(solution)/shard_map/ppermute | solution.py:21
  107.2 17.9 %collective-permute-start.4 = (bf16[256,1024]{1,0:T(8,128)(2,1)S(1)}, bf16[256,1024]{1,0:T(8,128)(2,1)S(1)}, u32[]{:S(2)}, u32[]{:S(2)}) collective-permute-start(bf16[256,1024]{1,0:T(8,128)(2,1)S(1)} %collective-permute-done.3), channel_id=1, source_target_pairs={{0,28},{4,0},{8,4},{12,8},{16,12},{20,16},{24,20},{28,24},{1,29},{... | collective-permute-start | bytes 1572872 | tf_op jit(solution)/shard_map/ppermute | solution.py:21
  125.1 19.3 %collective-permute-start.5 = (bf16[256,1024]{1,0:T(8,128)(2,1)S(1)}, bf16[256,1024]{1,0:T(8,128)(2,1)}, u32[]{:S(2)}, u32[]{:S(2)}) collective-permute-start(bf16[256,1024]{1,0:T(8,128)(2,1)S(1)} %collective-permute-done.4), channel_id=1, source_target_pairs={{0,28},{4,0},{8,4},{12,8},{16,12},{20,16},{24,20},{28,24},{1,29},{... | collective-permute-start | bytes 1572872 | tf_op jit(solution)/shard_map/ppermute | solution.py:21
  133.4 37.8 %copy-start.2 = (f32[2048]{0:T(1024)S(1)}, f32[2048]{0:T(1024)}, u32[]{:S(2)}) copy-start(f32[2048]{0:T(1024)} %param.7) | copy-start | bytes 24580
  144.4 18.2 %collective-permute-start.6 = (bf16[256,1024]{1,0:T(8,128)(2,1)}, bf16[256,1024]{1,0:T(8,128)(2,1)S(1)}, u32[]{:S(2)}, u32[]{:S(2)}) collective-permute-start(bf16[256,1024]{1,0:T(8,128)(2,1)} %collective-permute-done.5), channel_id=1, source_target_pairs={{0,28},{4,0},{8,4},{12,8},{16,12},{20,16},{24,20},{28,24},{1,29},{... | collective-permute-start | bytes 1572872 | tf_op jit(solution)/shard_map/ppermute | solution.py:21
  181.2 97.4 %copy-start.1 = (f32[512]{0:T(512)S(1)}, f32[512]{0:T(512)}, u32[]{:S(2)}) copy-start(f32[512]{0:T(512)} %param.11) | copy-start | bytes 6148
Sparse Core Ops, SparseCore 0:
  9.5 110.5 all-gather.2
  122.1 90.8 all-gather.4
  228.7 42.5 reduce-scatter.1
